TPU v7x, 32 devices: a whole 2x2x4 slice. The times are simulated.
32 devices in a mesh: ep: 8 (over z, x), tp: 4 (over y, core).
Axes of the slice: x: 2, y: 2, z: 4, core: 2. Of those that a mesh axis runs over, the one named last changes fastest.
Arguments:
- tokens: bfloat16 [4608, 2048], P(('ep', 'tp')), may hold values from -6 to 6
- norm_gain: float32 [2048], replicated, may hold values from 0.1 to 1.9
- expert_ids: int32 [4608, 8], P(('ep', 'tp')), may hold values from 0 to 15, all different within a row; in each aligned block of 144 rows (0 to 143, 144 to 287, ...) at most 144 rows name the same one
- route_weights: float32 [4608, 8], P(('ep', 'tp')), may hold values from 0.3 to 1
- expert_gate: bfloat16 [16, 512, 2048], P('ep', 'tp'), may hold values from -0.125 to 0.125
- expert_up: bfloat16 [16, 512, 2048], P('ep', 'tp'), may hold values from -0.125 to 0.125
- expert_down: bfloat16 [16, 512, 2048], P('ep', 'tp'), may hold values from -0.25 to 0.25
- shared_gate: bfloat16 [512, 2048], P('tp'), may hold values from -0.125 to 0.125
- shared_up: bfloat16 [512, 2048], P('tp'), may hold values from -0.125 to 0.125
- shared_down: bfloat16 [512, 2048], P('tp'), may hold values from -0.25 to 0.25
- side_in: bfloat16 [2048, 1024], P('ep'), may hold values from -0.125 to 0.125
- side_out: bfloat16 [2048, 1024], P('ep'), may hold values from -0.1875 to 0.1875
- side_gate: bfloat16 [2048], replicated, may hold values from -0.125 to 0.125
Outputs:
- mixed: bfloat16 [4608, 2048], P(('ep', 'tp'))
Inputs may be any that keep to these rules, and one draw needn't show every extreme that they name: `expert_ids`: each row names 8 different experts of 0 to 15; within the rows of one device (aligned blocks of 144 rows) no expert is named more than 144 times, and in some of those blocks some expert is named exactly 144 times.
All inputs are finite; a program needn't handle non-finite values.
Results may differ from a plain program's by a relative error of at most 0.0068.
Values may be sent and summed in bfloat16 or wider, within the bound.
No kernel may reach another device: no remote copies, remote signals or barrier semaphores. Data moves between devices by JAX's collectives and lax.ppermute only.
A program may use at most 320 MiB of HBM per device.

v0:
```python
import jax
import jax.numpy as jnp
from jax import lax
from jax.sharding import PartitionSpec as P

norm_eps = 1.0


def normalize(tokens, norm_gain):
    values = tokens.astype(jnp.float32)
    scale_inv = lax.rsqrt(jnp.mean(values * values, axis=-1, keepdims=True) + norm_eps)
    return (values * scale_inv * norm_gain).astype(jnp.bfloat16)


def swiglu(gate_part, up_part):
    return (jax.nn.silu(gate_part) * up_part).astype(jnp.bfloat16)


def body(
    tokens,
    norm_gain,
    expert_ids,
    route_weights,
    expert_gate,
    expert_up,
    expert_down,
    shared_gate,
    shared_up,
    shared_down,
    side_in,
    side_out,
    side_gate,
):
    normed = normalize(tokens, norm_gain)
    tok_count, width = normed.shape
    top_count = expert_ids.shape[1]
    groups = lax.axis_size("ep")
    local_experts = expert_gate.shape[0]
    experts_all = groups * local_experts
    capacity = 2 * tok_count * top_count // experts_all
    pair_count = tok_count * top_count
    flat_ids = expert_ids.reshape(pair_count)
    one_hot = (flat_ids[:, None] == jnp.arange(experts_all, dtype=jnp.int32)[None, :]).astype(
        jnp.int32
    )
    earlier = jnp.cumsum(one_hot, axis=0) - 1
    slot_of = jnp.sum(one_hot * earlier, axis=1)
    position = flat_ids * capacity + slot_of
    source_row = jnp.arange(pair_count, dtype=jnp.int32) // top_count
    buffers = (
        jnp.zeros((experts_all * capacity, width), jnp.bfloat16)
        .at[position]
        .set(normed[source_row])
    )
    buffers = buffers.reshape(groups, local_experts, capacity, width)
    received = lax.all_to_all(buffers, "ep", split_axis=0, concat_axis=0, tiled=True)
    gate_piece = lax.all_gather(expert_gate, "tp", axis=1, tiled=True)
    up_piece = lax.all_gather(expert_up, "tp", axis=1, tiled=True)
    down_piece = lax.all_gather(expert_down, "tp", axis=1, tiled=True)
    gate_part = jnp.einsum(
        "secd,efd->secf", received, gate_piece, preferred_element_type=jnp.float32
    )
    up_part = jnp.einsum("secd,efd->secf", received, up_piece, preferred_element_type=jnp.float32)
    hidden = swiglu(gate_part, up_part)
    total = jnp.einsum("secf,efd->secd", hidden, down_piece, preferred_element_type=jnp.float32)
    returned = lax.all_to_all(
        total.astype(jnp.bfloat16), "ep", split_axis=0, concat_axis=0, tiled=True
    )
    picked = returned.reshape(experts_all * capacity, width)[position]
    weighted = picked.astype(jnp.float32) * route_weights.reshape(pair_count, 1)
    routed = jnp.sum(weighted.reshape(tok_count, top_count, width), axis=1)
    gate_piece = lax.all_gather(shared_gate, "tp", axis=0, tiled=True)
    up_piece = lax.all_gather(shared_up, "tp", axis=0, tiled=True)
    down_piece = lax.all_gather(shared_down, "tp", axis=0, tiled=True)
    gate_part = jnp.einsum("td,fd->tf", normed, gate_piece, preferred_element_type=jnp.float32)
    up_part = jnp.einsum("td,fd->tf", normed, up_piece, preferred_element_type=jnp.float32)
    hidden = swiglu(gate_part, up_part)
    shared = jnp.dot(hidden, down_piece, preferred_element_type=jnp.float32)
    whole_in, whole_out = (
        lax.all_gather(side_in, "ep", axis=0, tiled=True),
        lax.all_gather(side_out, "ep", axis=0, tiled=True),
    )
    side_hidden = jax.nn.silu(jnp.dot(normed, whole_in, preferred_element_type=jnp.float32)).astype(
        jnp.bfloat16
    )
    side_value = jnp.einsum("ts,ds->td", side_hidden, whole_out, preferred_element_type=jnp.float32)
    opening = jax.nn.sigmoid(jnp.dot(normed, side_gate, preferred_element_type=jnp.float32))
    return (routed + shared + opening[:, None] * side_value).astype(jnp.bfloat16)


def solution(mesh):
    placed = (
        P(("ep", "tp"), None),
        P(),
        P(("ep", "tp"), None),
        P(("ep", "tp"), None),
        P("ep", "tp", None),
        P("ep", "tp", None),
        P("ep", "tp", None),
        P("tp", None),
        P("tp", None),
        P("tp", None),
        P("ep", None),
        P("ep", None),
        P(),
    )
    return jax.shard_map(
        body, mesh=mesh, in_specs=placed, out_specs=P(("ep", "tp"), None), check_vma=False
    )
```

profile of v0, /device:TPU:0, one launch (start us, length us, event | category | flops | bytes accessed | tf_op | source)
XLA Modules:
  0.0 640.6 jit_solution(15951848686888456871)
XLA Ops:
  6.5 0.7 all-gather.11.cloned.1.call-update
  7.3 0.0 all-gather.9.cloned.1.call-start
  7.3 0.7 all-gather.9.cloned.1.call-update
  8.0 0.8 copy.22
  8.8 0.1 eq.29
  8.9 0.1 eq.25
  9.0 4.6 reduce-window.6
  13.6 0.4 slice_reduce_fusion
  14.0 0.2 reduce-window.9
  14.2 0.7 broadcast_multiply_fusion
  14.9 0.1 copy.21
  15.0 0.1 mul.71
  15.2 0.1 add_add_fusion
  15.4 1.3 fusion.21
  16.6 0.9 fusion.23
  17.5 35.8 %scatter_custom_fusion = bf16[2304,2048]{1,0:T(8,128)(2,1)} fusion(s32[1152]{0:T(1024)S(1)} %fusion.35, bf16[144,2048]{1,0:T(8,128)(2,1)S(1)} %fusion.23, s32[2048]{0:T(1024)S(1)} %pad_clamp_fusion.1, bf16[]{:T(256)} %constant.35.clone.1), kind=kCustom, calls=%fused_computation.17 | custom fusion | bytes 9437186 | tf_op jit(solution)/shard_map/scatter | solution.py:53
  53.3 7.3 %all-to-all-start = ((bf16[8,2,144,2048]{3,2,1,0:T(8,128)(2,1)}), bf16[8,2,144,2048]{3,2,1,0:T(8,128)(2,1)}, u32[]{:S(2)}, u32[]{:S(2)}) async-start(bf16[8,2,144,2048]{3,2,1,0:T(8,128)(2,1)} %bitcast.67), calls=%async_computation | async-start | bytes 18874368 | tf_op jit(solution)/shard_map/all_to_all | solution.py:56
  60.7 0.0 all-gather.13.cloned.1.call-start
  60.7 0.7 all-gather.13.cloned.1.call-update
  61.4 0.0 all-gather.15.cloned.1.call-start
  61.4 0.5 all-gather.15.cloned.1.call-update
  62.0 0.0 all-gather.17.cloned.1.call-start
  62.0 0.5 all-gather.17.cloned.1.call-update
  62.5 0.0 all-gather.19.cloned.1.call-start
  62.6 0.5 all-gather.19.cloned.1.call-update
  63.1 0.0 all-gather.11.cloned.1.call-done
  63.2 203.1 %all-to-all-done = bf16[8,2,144,2048]{3,2,1,0:T(8,128)(2,1)} async-done(((bf16[8,2,144,2048]{3,2,1,0:T(8,128)(2,1)}), bf16[8,2,144,2048]{3,2,1,0:T(8,128)(2,1)}, u32[]{:S(2)}, u32[]{:S(2)}) %all-to-all-start) | async-done | bytes 9437216 | tf_op jit(solution)/shard_map/all_to_all | solution.py:56
  266.3 10.3 %fusion.1 = f32[2,8,144,512]{3,2,1,0:T(8,128)} fusion(bf16[8,2,144,2048]{3,2,1,0:T(8,128)(2,1)} %all-to-all-done, bf16[2,512,2048]{2,1,0:T(8,128)(2,1)} %all-gather.11.cloned.1.call-done), kind=kOutput, calls=%fused_computation.6 | convolution fusion | flops 4831838208 | bytes 18350080 | tf_op jit(solution)/shard_map/secd,efd->secf/dot_general | solution.py:63
  276.6 10.2 %fusion.5 = bf16[8,2,144,512]{3,2,0,1:T(8,128)(2,1)S(1)} fusion(f32[2,8,144,512]{3,2,1,0:T(8,128)} %fusion.1, bf16[2,512,2048]{2,1,0:T(8,128)(2,1)} %all-gather.9.cloned.1.call-done, bf16[8,2,144,2048]{3,2,1,0:T(8,128)(2,1)} %all-to-all-done), kind=kOutput, calls=%fused_computation.11 | convolution fusion | flops 4838916096 | bytes 20709376 | tf_op jit(solution)/shard_map/secd,efd->secf/dot_general | solution.py:60
  286.8 9.6 %convert_bitcast_fusion = bf16[8,2,144,2048]{3,2,0,1:T(8,128)(2,1)} fusion(bf16[8,2,144,512]{3,2,0,1:T(8,128)(2,1)S(1)} %fusion.5, bf16[2,512,2048]{2,1,0:T(8,128)(2,1)} %all-gather.13.cloned.1.call-done), kind=kOutput, calls=%fused_computation.5 | convolution fusion | flops 4836556800 | bytes 15990784 | tf_op jit(solution)/shard_map/secf,efd->secd/dot_general | solution.py:65
  296.5 9.3 %copy.26 = bf16[8,2,144,2048]{3,2,1,0:T(8,128)(2,1)} copy(bf16[8,2,144,2048]{3,2,0,1:T(8,128)(2,1)} %convert_bitcast_fusion) | data formatting | bytes 18874368 | tf_op jit(solution)/shard_map/convert_element_type | solution.py:67
  305.7 5.2 all-to-all-start.1
  310.9 0.0 all-gather.21.cloned.1.call-start
  310.9 0.7 all-gather.21.cloned.1.call-update
  311.7 0.3 all-gather.23.cloned.1.call-start
  311.9 0.4 all-gather.23.cloned.1.call-update
  312.4 0.1 copy.27
  312.6 0.3 fusion.42
  312.8 0.0 all-gather.15.cloned.1.call-done
  312.8 2.4 fusion.41
  315.3 267.8 %all-to-all-done.1 = bf16[8,2,144,2048]{3,2,1,0:T(8,128)(2,1)} async-done(((bf16[8,2,144,2048]{3,2,1,0:T(8,128)(2,1)}), bf16[8,2,144,2048]{3,2,1,0:T(8,128)(2,1)}, u32[]{:S(2)}, u32[]{:S(2)}) %all-to-all-start.1) | async-done | bytes 9437216 | tf_op jit(solution)/shard_map/all_to_all | solution.py:66
  583.0 15.5 %gather_fusion = bf16[1152,2048]{1,0:T(8,128)(2,1)} fusion(bf16[2304,2048]{1,0:T(8,128)(2,1)} %bitcast.11, s32[2048]{0:T(1024)S(1)} %pad_clamp_fusion), kind=kCustom, calls=%fused_computation.1 | custom fusion | bytes 9441792 | tf_op jit(solution)/shard_map/gather | solution.py:69
  598.6 7.0 %fusion = f32[144,2048]{1,0:T(8,128)S(1)} fusion(bf16[1152,2048]{1,0:T(8,128)(2,1)} %gather_fusion, f32[144,8]{1,0:T(8,128)S(1)} %copy.27), kind=kLoop, calls=%fused_computation.4 | loop fusion | flops 6782976 | bytes 5902848 | tf_op jit(solution)/shard_map/reduce_sum | solution.py:71
  605.6 0.0 all-gather.17.cloned.1.call-done
  605.7 3.5 convolution_add_fusion
  609.2 0.0 all-gather.21.cloned.1.call-done
  609.2 17.7 %all-gather.23.cloned.1.call-done = bf16[2048,1024]{1,0:T(8,128)(2,1)} async-done(((bf16[256,1024]{1,0:T(8,128)(2,1)}), bf16[2048,1024]{1,0:T(8,128)(2,1)}) %all-gather.23.cloned.1.call-update) | async-done | bytes 4194320 | tf_op jit(solution)/shard_map/all_gather | solution.py:81
  626.9 6.5 %fusion.16 = bf16[144,2048]{1,0:T(8,128)(2,1)} fusion(f32[144,2048]{1,0:T(8,128)S(1)} %convolution_add_fusion, bf16[2048,1024]{1,0:T(8,128)(2,1)} %all-gather.23.cloned.1.call-done, f32[144]{0:T(256)S(1)} %add_divide_fusion, bf16[144,2048]{1,0:T(8,128)(2,1)S(1)} %fusion.23, bf16[2048,1024]{1,0:T(8,128)(2,1)} %all-gather.21.cloned.1.call-done), kind=kOutput, calls=%fused_computation.26 | convolution fusion | flops 1209581568 | bytes 10748480 | tf_op jit(solution)/shard_map/ts,ds->td/dot_general | solution.py:86
  (19 shorter events, 0.2 us)
Async XLA Ops:
  6.5 10.1 %copy-start = (bf16[144,2048]{1,0:T(8,128)(2,1)S(1)}, bf16[144,2048]{1,0:T(8,128)(2,1)}, u32[]{:S(2)}) copy-start(bf16[144,2048]{1,0:T(8,128)(2,1)} %param.13) | copy-start | bytes 1769476
  6.5 56.6 %all-gather.11.cloned.1.call-start = ((), (), s32[]{:S(2)}) async-start(), calls=%async_computation.3 | async-start | bytes 5242880 | tf_op jit(solution)/shard_map/all_gather | solution.py:58
  7.3 269.4 %all-gather.9.cloned.1.call-start = ((), (), s32[]{:S(2)}) async-start(), calls=%async_computation.2 | async-start | bytes 5242880 | tf_op jit(solution)/shard_map/all_gather | solution.py:57
  53.3 213.0 %all-to-all-start = ((bf16[8,2,144,2048]{3,2,1,0:T(8,128)(2,1)}), bf16[8,2,144,2048]{3,2,1,0:T(8,128)(2,1)}, u32[]{:S(2)}, u32[]{:S(2)}) async-start(bf16[8,2,144,2048]{3,2,1,0:T(8,128)(2,1)} %bitcast.67), calls=%async_computation | async-start | bytes 18874368 | tf_op jit(solution)/shard_map/all_to_all | solution.py:56
  60.7 226.2 %all-gather.13.cloned.1.call-start = ((), (), s32[]{:S(2)}) async-start(), calls=%async_computation.4 | async-start | bytes 5242880 | tf_op jit(solution)/shard_map/all_gather | solution.py:59
  61.4 251.5 %all-gather.15.cloned.1.call-start = ((), (), s32[]{:S(2)}) async-start(), calls=%async_computation.5 | async-start | bytes 2621440 | tf_op jit(solution)/shard_map/all_gather | solution.py:72
  62.0 543.7 %all-gather.17.cloned.1.call-start = ((), (), s32[]{:S(2)}) async-start(), calls=%async_computation.6 | async-start | bytes 2621440 | tf_op jit(solution)/shard_map/all_gather | solution.py:73
  62.5 543.1 %all-gather.19.cloned.1.call-start = ((), (), s32[]{:S(2)}) async-start(), calls=%async_computation.7 | async-start | bytes 2621440 | tf_op jit(solution)/shard_map/all_gather | solution.py:74
  305.7 6.7 %copy-start.1 = (f32[144,8]{0,1:T(8,128)S(1)}, f32[144,8]{0,1:T(8,128)}, u32[]{:S(2)}) copy-start(f32[144,8]{0,1:T(8,128)} %param.16) | copy-start | bytes 13828
  305.7 6.8 %copy-start.2 = (bf16[2048]{0:T(1024)(128)(2,1)S(1)}, bf16[2048]{0:T(1024)(128)(2,1)}, u32[]{:S(2)}) copy-start(bf16[2048]{0:T(1024)(128)(2,1)} %param.25) | copy-start | bytes 12292
  305.7 277.3 %all-to-all-start.1 = ((bf16[8,2,144,2048]{3,2,1,0:T(8,128)(2,1)}), bf16[8,2,144,2048]{3,2,1,0:T(8,128)(2,1)}, u32[]{:S(2)}, u32[]{:S(2)}) async-start(bf16[8,2,144,2048]{3,2,1,0:T(8,128)(2,1)} %copy.26), calls=%async_computation.1 | async-start | bytes 18874368 | tf_op jit(solution)/shard_map/all_to_all | solution.py:66
  310.9 298.3 %all-gather.21.cloned.1.call-start = ((), (), s32[]{:S(2)}) async-start(), calls=%async_computation.8 | async-start | bytes 4718592 | tf_op jit(solution)/shard_map/all_gather | solution.py:80
  311.7 315.3 %all-gather.23.cloned.1.call-start = ((), (), s32[]{:S(2)}) async-start(), calls=%async_computation.9 | async-start | bytes 4718592 | tf_op jit(solution)/shard_map/all_gather | solution.py:81
Sparse Core Ops, SparseCore 0:
  8.9 37.1 all-gather.10
  47.7 34.4 all-gather.8
  83.7 34.4 all-gather.12
  119.7 22.5 all-gather.14
  143.7 22.5 all-gather.16
  167.7 22.5 all-gather.18
  313.8 219.9 all-gather.20
  536.0 90.8 all-gather.22
where the time goes:
time: 644 us; the launch traced here: 641 us
  waiting for transfers between devices  494 us (77%)
  local copies, waits for them, and re-layouts  62.3 us (10%)
  matrix products  42.8 us (7%)
  other arithmetic  14.8 us (2%)
  between operations  14.1 us (2%)
  starting transfers between devices  13 us (2%)
    all_to_all x1, waiting for transfers between devices, body(): lax.all_to_all(total.astype(jnp.bfloat16), 'ep', split_axis=0, concat_axi...  268 us
    all_to_all x1, waiting for transfers between devices, body(): lax.all_to_all(buffers, 'ep', split_axis=0, concat_axis=0, tiled=True)  203 us
    scatter x1, local copies, waits for them, and re-layouts, body(): buffers = jnp.zeros((experts_all * capacity, width), jnp.bfloat16).at[pos...  35.8 us
    all_gather x1, waiting for transfers between devices, body(): lax.all_gather(side_out, 'ep', axis=0, tiled=True)  17.7 us
    gather x1, local copies, waits for them, and re-layouts, body(): picked = returned.reshape(experts_all * capacity, width)[position]  15.5 us
  transfers between devices with their start and end apart: 10, of which 3 were waited for; matrix products, arithmetic and copies ran while one was open for 18% of the time, Pallas kernels for 0%

commit v1 on v0

v1 whole, which is shorter than its diff:
```python
import jax
import jax.numpy as jnp
from jax import lax
from jax.sharding import PartitionSpec as P

norm_eps = 1.0
cores = 2


def normalize(tokens, norm_gain):
    values = tokens.astype(jnp.float32)
    scale_inv = lax.rsqrt(jnp.mean(values * values, axis=-1, keepdims=True) + norm_eps)
    return (values * scale_inv * norm_gain).astype(jnp.bfloat16)


def over_y(piece):
    size = lax.axis_size("tp")
    places = size // cores
    return [
        lax.ppermute(
            piece,
            "tp",
            [(s, (s // cores + r) % places * cores + s % cores) for s in range(size)],
        )
        for r in range(1, places)
    ]


def over_core(piece):
    size = lax.axis_size("tp")
    return lax.ppermute(piece, "tp", [(s, s // cores * cores + (s + 1) % cores) for s in range(size)])


def rows_dot(left, right):
    return lax.dot_general(
        left, right, (((1,), (1,)), ((), ())), preferred_element_type=jnp.float32
    )


def body(
    tokens,
    norm_gain,
    expert_ids,
    route_weights,
    expert_gate,
    expert_up,
    expert_down,
    shared_gate,
    shared_up,
    shared_down,
    side_in,
    side_out,
    side_gate,
):
    groups = lax.axis_size("ep")
    rank = lax.axis_index("ep")
    local_experts, hidden_part, width = expert_gate.shape
    experts_all = groups * local_experts

    normed = normalize(tokens, norm_gain)
    every = lax.all_gather(normed, "ep", axis=0, tiled=True)

    chosen = expert_ids[:, :, None] == jnp.arange(experts_all, dtype=jnp.int32)[None, None, :]
    dense = jnp.sum(jnp.where(chosen, route_weights[:, :, None], 0.0), axis=1)
    opening = jax.nn.sigmoid(jnp.dot(normed, side_gate, preferred_element_type=jnp.float32))
    factors = lax.all_gather(
        jnp.concatenate([dense, opening[:, None]], axis=1), "ep", axis=0, tiled=True
    )
    mine = lax.dynamic_slice_in_dim(factors, rank * local_experts, local_experts, axis=1)
    opened = factors[:, experts_all:]

    flat = [w.reshape(local_experts * hidden_part, width) for w in (expert_gate, expert_up, expert_down)]
    far = [over_y(w) for w in flat]
    near = [[w, over_core(w)] for w in flat]
    far = [[q for p in w for q in (p, over_core(p))] for w in far]

    unit_count = shared_gate.shape[0] // groups
    shared_units = jnp.stack(
        [
            lax.dynamic_slice_in_dim(w, rank * unit_count, unit_count, axis=0)
            for w in (shared_gate, shared_up, shared_down)
        ]
    )
    shared_units = lax.all_gather(shared_units, "tp", axis=1, tiled=True)

    side_units = side_in.shape[1] // groups
    both = jnp.stack([side_in, side_out]).reshape(2, side_in.shape[0], groups, side_units)
    both = lax.all_to_all(both, "ep", split_axis=2, concat_axis=1, tiled=True)
    both = both.reshape(2, width, side_units)

    def routed_hidden(gate, up):
        gate_part, up_part = rows_dot(every, gate), rows_dot(every, up)
        place = lax.broadcasted_iota(jnp.int32, (1, gate.shape[0]), 1) // hidden_part % local_experts
        scale = mine[:, 0:1]
        for e in range(1, local_experts):
            scale = jnp.where(place == e, mine[:, e : e + 1], scale)
        return (jax.nn.silu(gate_part) * up_part * scale).astype(jnp.bfloat16)

    near_gate, near_up, near_down = [jnp.concatenate(w) for w in near]
    far_gate, far_up, far_down = [jnp.concatenate(w) for w in far]

    hidden = routed_hidden(near_gate, near_up)
    total = jnp.dot(hidden, near_down, preferred_element_type=jnp.float32)
    shared_hidden = (
        jax.nn.silu(rows_dot(every, shared_units[0])) * rows_dot(every, shared_units[1])
    ).astype(jnp.bfloat16)
    total += jnp.dot(shared_hidden, shared_units[2], preferred_element_type=jnp.float32)
    side_hidden = (
        jax.nn.silu(jnp.dot(every, both[0], preferred_element_type=jnp.float32)) * opened
    ).astype(jnp.bfloat16)
    total += rows_dot(side_hidden, both[1])
    hidden = routed_hidden(far_gate, far_up)
    total += jnp.dot(hidden, far_down, preferred_element_type=jnp.float32)
    return lax.psum_scatter(total.astype(jnp.bfloat16), "ep", scatter_dimension=0, tiled=True)


def solution(mesh):
    placed = (
        P(("ep", "tp"), None),
        P(),
        P(("ep", "tp"), None),
        P(("ep", "tp"), None),
        P("ep", "tp", None),
        P("ep", "tp", None),
        P("ep", "tp", None),
        P("tp", None),
        P("tp", None),
        P("tp", None),
        P("ep", None),
        P("ep", None),
        P(),
    )
    return jax.shard_map(
        body, mesh=mesh, in_specs=placed, out_specs=P(("ep", "tp"), None), check_vma=False
    )
```

time: 644 us -> 285 us (0.44)
  waiting for transfers between devices: 494 us -> 109 us
  blocking collectives: 0 us -> 73.8 us
  local copies, waits for them, and re-layouts: 62.3 us -> 3.53 us
  matrix products: 42.8 us -> 68.7 us
  other arithmetic: 14.8 us -> 3.66 us
    all_to_all x2 -> x1, waiting for transfers between devices: 471 us -> 0.01 us  [body(): both = lax.all_to_all(both, 'ep', split_axis=2, concat_axis=1, tiled=True)]
    reduce_scatter x0 -> x1, waiting for transfers between devices: none -> 94.2 us  [body(): lax.psum_scatter(total.astype(jnp.bfloat16), 'ep', scatter_dimension=0, t...]
    all_gather x0 -> x2, blocking collectives: none -> 73.8 us  [the longest x1 64.5 us: body(): lax.all_gather(jnp.concatenate([dense, opening[:, None]], axis=1), 'ep',...]
    scatter x1 -> x0, local copies, waits for them, and re-layouts: 35.8 us -> none  [body(): buffers = jnp.zeros((experts_all * capacity, width), jnp.bfloat16).at[pos...]
    dot_general x6 -> x7, matrix products: 42.5 us -> 68.5 us  [the longest x4 28.8 us: rows_dot(): lax.dot_general(left, right, (((1,), (1,)), ((), ())), preferred_element_...]
    gather x1 -> x0, local copies, waits for them, and re-layouts: 15.5 us -> none  [body(): picked = returned.reshape(experts_all * capacity, width)[position]]
    convert_element_type x1 -> x0, local copies, waits for them, and re-layouts: 9.26 us -> none  [body(): total.astype(jnp.bfloat16)]
    reduce_sum x2 -> x1, other arithmetic: 7.05 us -> 0.02 us  [body(): dense = jnp.sum(jnp.where(chosen, route_weights[:, :, None], 0.0), axis=1)]
  transfers between devices with their start and end apart: 10 -> 12, of which waited for: 3 -> 2; matrix products, arithmetic and copies ran while one was open for 18% -> 19% of each run, Pallas kernels for 0% -> 0%
where the time goes in v1:
time: 285 us
  waiting for transfers between devices  109 us (38%)
  blocking collectives  73.8 us (26%)
  matrix products  68.7 us (24%)
  between operations  13.6 us (5%)
  starting transfers between devices  12.2 us (4%)
  other arithmetic  3.66 us (1%)
  local copies, waits for them, and re-layouts  3.53 us (1%)
    reduce_scatter x1, waiting for transfers between devices, body(): lax.psum_scatter(total.astype(jnp.bfloat16), 'ep', scatter_dimension=0, t...  94.2 us
    all_gather x1, blocking collectives, body(): lax.all_gather(jnp.concatenate([dense, opening[:, None]], axis=1), 'ep',...  64.5 us
    dot_general x4, matrix products, rows_dot(): lax.dot_general(left, right, (((1,), (1,)), ((), ())), preferred_element_...  28.8 us
    dot_general x1, matrix products, body(): total += jnp.dot(hidden, far_down, preferred_element_type=jnp.float32)  17.3 us
    all_gather x1, waiting for transfers between devices, body(): every = lax.all_gather(normed, 'ep', axis=0, tiled=True)  15.1 us
    dot_general x1, matrix products, body(): total = jnp.dot(hidden, near_down, preferred_element_type=jnp.float32)  13.5 us
    all_gather x1, blocking collectives, body(): shared_units = lax.all_gather(shared_units, 'tp', axis=1, tiled=True)  9.29 us
    dot_general x1, matrix products, body(): jnp.dot(shared_hidden, shared_units[2], preferred_element_type=jnp.float32)  8.95 us
  transfers between devices with their start and end apart: 12, of which 2 were waited for; matrix products, arithmetic and copies ran while one was open for 19% of the time, Pallas kernels for 0%

profile of v1, /device:TPU:0, one launch (start us, length us, event | category | flops | bytes accessed | tf_op | source)
XLA Modules:
  0.0 285.0 jit_solution(7317867173243975410)
XLA Ops:
  6.5 1.4 fusion.32
  7.9 2.1 fusion.34
  10.0 0.0 all-gather.3.cloned.1.call-update
  10.1 3.1 %collective-permute-start.3 = (bf16[256,2048]{1,0:T(8,128)(2,1)}, bf16[256,2048]{1,0:T(8,128)(2,1)}, u32[]{:S(2)}, u32[]{:S(2)}) collective-permute-start(bf16[256,2048]{1,0:T(8,128)(2,1)} %bitcast), channel_id=1, source_target_pairs={{0,2},{1,3},{2,0},{3,1},{4,6},{5,7},{6,4},{7,5},{8,10},{9,11},{10,... | collective-permute-start | bytes 3145736 | tf_op jit(solution)/shard_map/ppermute | solution.py:20
  13.1 0.0 collective-permute-start
  13.1 0.2 collective-permute-start.5
  13.3 0.4 collective-permute-start.1
  13.6 0.2 copy.38
  13.8 0.2 copy.39
  14.1 0.1 pad_maximum_fusion
  14.2 0.0 copy-start.6
  14.2 0.0 copy-start.7
  14.2 0.0 copy-start.8
  14.2 0.0 copy-start.2
  14.2 1.0 copy.40
  15.2 6.0 %all-to-all-start = ((bf16[2,256,8,128]{1,3,0,2:T(8,128)(2,1)}), bf16[2,256,8,128]{1,3,0,2:T(8,128)(2,1)S(1)}, u32[]{:S(2)}, u32[]{:S(2)}) async-start(bf16[2,256,8,128]{1,3,0,2:T(8,128)(2,1)} %copy.40), calls=%async_computation | async-start | bytes 2097152 | tf_op jit(solution)/shard_map/all_to_all | solution.py:88
  21.3 0.0 reduce-scatter.2.cloned.1.call-start
  21.3 1.6 collective-permute-start.7
  23.0 0.3 fusion.73
  23.3 64.5 %all-gather = f32[8,144,17]{1,2,0:T(8,128)S(1)} all-gather(f32[1,144,17]{1,2,0:T(8,128)S(1)} %maximum_bitcast_fusion), channel_id=1, replica_groups=mesh['ep'=8,'tp'=4] {'ep'}, dimensions={0}, use_global_device_ids=true | all-gather | bytes 88128 | tf_op jit(solution)/shard_map/all_gather | solution.py:66
  87.8 0.1 reshape.91
  88.0 0.0 collective-permute-done.3
  88.1 0.1 collective-permute-start.4
  88.1 0.9 dynamic-slice_bitcast_fusion
  89.1 9.3 %all_gather.11 = bf16[3,64,2048]{2,1,0:T(8,128)(2,1)} all-gather(bf16[3,16,2048]{2,1,0:T(8,128)(2,1)S(1)} %pad_maximum_fusion.1), channel_id=1, replica_groups=mesh['ep'=8,'tp'=4] {'tp'}, dimensions={1}, use_global_device_ids=true | all-gather | bytes 983040 | tf_op jit(solution)/shard_map/all_gather | solution.py:84
  98.4 0.0 all-to-all-done
  98.4 0.8 copy.41
  99.2 0.1 fusion.70
  99.3 0.0 collective-permute-done.5
  99.3 0.4 collective-permute-start.2
  99.7 0.0 collective-permute-done.7
  99.7 0.2 collective-permute-start.6
  99.9 0.0 collective-permute-done.4
  99.9 0.4 collective-permute-start.8
  100.2 15.1 %all-gather.3.cloned.1.call-done = bf16[1152,2048]{1,0:T(8,128)(2,1)} async-done(((bf16[144,2048]{1,0:T(8,128)(2,1)}), bf16[1152,2048]{1,0:T(8,128)(2,1)}) %all-gather.3.cloned.1.call-update) | async-done | bytes 4718608 | tf_op jit(solution)/shard_map/all_gather | solution.py:61
  115.3 7.0 %fusion.17 = f32[1152,512]{1,0:T(8,128)} fusion(bf16[1152,2048]{1,0:T(8,128)(2,1)} %all-gather.3.cloned.1.call-done, bf16[256,2048]{1,0:T(8,128)(2,1)} %collective-permute-done.4, bf16[256,2048]{1,0:T(8,128)(2,1)} %collective-permute-done.3), kind=kOutput, calls=%fused_computation.19 | convolution fusion | flops 2420113408 | bytes 9175040 | tf_op jit(solution)/shard_map/dot_general | solution.py:35
  122.3 10.9 %fusion.45 = f32[1152,2048]{1,0:T(8,128)} fusion(bf16[2048,128]{1,0:T(8,128)(2,1)S(1)} %bitcast.45, f32[1152]{0:T(1024)S(1)} %get-tuple-element.6, bf16[1152,2048]{1,0:T(8,128)(2,1)} %all-gather.3.cloned.1.call-done, bf16[2048,128]{1,0:T(8,128)(2,1)S(1)} %bitcast.44), kind=kOutput, calls=%fused_computation.45 | convolution fusion | flops 1208844288 | bytes 15208960 | tf_op jit(solution)/shard_map/dot_general | solution.py:35
  133.3 3.9 %fusion.53 = f32[1152,64]{0,1:T(8,128)S(1)} fusion(bf16[1152,2048]{1,0:T(8,128)(2,1)} %all-gather.3.cloned.1.call-done, bf16[3,64,2048]{2,1,0:T(8,128)(2,1)S(1)} %copy-done.3), kind=kOutput, calls=%fused_computation.56 | convolution fusion | flops 301989888 | bytes 5275648 | tf_op jit(solution)/shard_map/dot_general | solution.py:35
  137.2 9.0 %fusion.44 = f32[1152,2048]{1,0:T(8,128)} fusion(bf16[1152,2048]{1,0:T(8,128)(2,1)} %all-gather.3.cloned.1.call-done, f32[1152,64]{0,1:T(8,128)S(1)} %fusion.53, bf16[3,64,2048]{2,1,0:T(8,128)(2,1)S(1)} %copy-done.3), kind=kOutput, calls=%fused_computation.42 | convolution fusion | flops 604422144 | bytes 14974976 | tf_op jit(solution)/shard_map/dot_general | solution.py:107
  146.1 0.0 collective-permute-done
  146.1 7.0 %fusion.3 = f32[1152,512]{1,0:T(8,128)} fusion(bf16[1152,2048]{1,0:T(8,128)(2,1)} %all-gather.3.cloned.1.call-done, bf16[256,2048]{1,0:T(8,128)(2,1)} %collective-permute-done, bf16[256,2048]{1,0:T(8,128)(2,1)} %bitcast), kind=kOutput, calls=%fused_computation.7 | convolution fusion | flops 2420113408 | bytes 9175040 | tf_op jit(solution)/shard_map/dot_general | solution.py:35
  153.1 0.0 collective-permute-done.1
  153.1 0.0 collective-permute-done.2
  153.1 13.5 %fusion.13 = f32[1152,2048]{1,0:T(8,128)} fusion(bf16[256,2048]{1,0:T(8,128)(2,1)} %collective-permute-done.2, bf16[256,2048]{1,0:T(8,128)(2,1)} %bitcast.5, f32[1152,512]{1,0:T(8,128)} %fusion.3, bf16[1152,2048]{1,0:T(8,128)(2,1)} %all-gather.3.cloned.1.call-done, bf16[256,2048]{1,0:T(8,128)(2,1)} %collective-permute-done.1, ...), kind=kOutput, calls=%fused_computation.15 | convolution fusion | flops 4844945408 | bytes 20719104 | tf_op jit(solution)/shard_map/dot_general | solution.py:103
  166.6 0.0 collective-permute-done.6
  166.6 17.3 %add_convert_fusion = bf16[1152,2048]{1,0:T(8,128)(2,1)} fusion(f32[1152,2048]{1,0:T(8,128)} %fusion.45, f32[1152,2048]{1,0:T(8,128)} %fusion.13, f32[1152,2048]{1,0:T(8,128)} %fusion.44, bf16[256,2048]{1,0:T(8,128)(2,1)} %collective-permute-done.8, bf16[256,2048]{1,0:T(8,128)(2,1)} %collective-permute-done.7, f32[1152,512]{1,0:T(8,128)} %fusion.17, ...), kind=kOutput, calls=%fused_computation | convolution fusion | flops 4854382592 | bytes 44312064 | tf_op jit(solution)/shard_map/dot_general | solution.py:113
  183.9 0.0 reduce-scatter.2.cloned.1.call-update
  183.9 94.2 %reduce-scatter.2.cloned.1.call-done = bf16[144,2048]{1,0:T(8,128)(2,1)} async-done(((bf16[1152,2048]{1,0:T(8,128)(2,1)}), bf16[144,2048]{1,0:T(8,128)(2,1)}) %reduce-scatter.2.cloned.1.call-update) | async-done | bytes 589840 | tf_op jit(solution)/shard_map/reduce_scatter | solution.py:114
  (26 shorter events, 0.2 us)
Async XLA Ops:
  6.5 81.5 %copy-start = (bf16[128,2048]{1,0:T(8,128)(2,1)S(1)}, bf16[128,2048]{1,0:T(8,128)(2,1)}, u32[]{:S(2)}) copy-start(bf16[128,2048]{1,0:T(8,128)(2,1)} %param.20) | copy-start | bytes 1572868
  6.5 7.1 %copy-start.4 = (bf16[256,1024]{1,0:T(8,128)(2,1)S(1)}, bf16[256,1024]{1,0:T(8,128)(2,1)}, u32[]{:S(2)}) copy-start(bf16[256,1024]{1,0:T(8,128)(2,1)} %param.23) | copy-start | bytes 1572868
  6.5 7.3 %copy-start.5 = (bf16[256,1024]{1,0:T(8,128)(2,1)S(1)}, bf16[256,1024]{1,0:T(8,128)(2,1)}, u32[]{:S(2)}) copy-start(bf16[256,1024]{1,0:T(8,128)(2,1)} %param.24) | copy-start | bytes 1572868
  6.5 108.8 %all-gather.3.cloned.1.call-start = ((), (), s32[]{:S(2)}) async-start(), calls=%async_computation.2 | async-start | bytes 5308416 | tf_op jit(solution)/shard_map/all_gather | solution.py:61
  10.1 78.0 %collective-permute-start.3 = (bf16[256,2048]{1,0:T(8,128)(2,1)}, bf16[256,2048]{1,0:T(8,128)(2,1)}, u32[]{:S(2)}, u32[]{:S(2)}) collective-permute-start(bf16[256,2048]{1,0:T(8,128)(2,1)} %bitcast), channel_id=1, source_target_pairs={{0,2},{1,3},{2,0},{3,1},{4,6},{5,7},{6,4},{7,5},{8,10},{9,11},{10,... | collective-permute-start | bytes 3145736 | tf_op jit(solution)/shard_map/ppermute | solution.py:20
  13.1 133.0 %collective-permute-start = (bf16[256,2048]{1,0:T(8,128)(2,1)}, bf16[256,2048]{1,0:T(8,128)(2,1)}, u32[]{:S(2)}, u32[]{:S(2)}) collective-permute-start(bf16[256,2048]{1,0:T(8,128)(2,1)} %bitcast), channel_id=1, source_target_pairs={{0,1},{1,0},{2,3},{3,2},{4,5},{5,4},{6,7},{7,6},{8,9},{9,8},{10,11... | collective-permute-start | bytes 3145736 | tf_op jit(solution)/shard_map/ppermute | solution.py:31
  13.1 86.2 %collective-permute-start.5 = (bf16[256,2048]{1,0:T(8,128)(2,1)}, bf16[256,2048]{1,0:T(8,128)(2,1)}, u32[]{:S(2)}, u32[]{:S(2)}) collective-permute-start(bf16[256,2048]{1,0:T(8,128)(2,1)} %bitcast.1), channel_id=1, source_target_pairs={{0,2},{1,3},{2,0},{3,1},{4,6},{5,7},{6,4},{7,5},{8,10},{9,11},{10,... | collective-permute-start | bytes 3145736 | tf_op jit(solution)/shard_map/ppermute | solution.py:20
  13.3 139.8 %collective-permute-start.1 = (bf16[256,2048]{1,0:T(8,128)(2,1)}, bf16[256,2048]{1,0:T(8,128)(2,1)}, u32[]{:S(2)}, u32[]{:S(2)}) collective-permute-start(bf16[256,2048]{1,0:T(8,128)(2,1)} %bitcast.1), channel_id=1, source_target_pairs={{0,1},{1,0},{2,3},{3,2},{4,5},{5,4},{6,7},{7,6},{8,9},{9,8},{10,11... | collective-permute-start | bytes 3145736 | tf_op jit(solution)/shard_map/ppermute | solution.py:31
  14.2 8.8 %copy-start.6 = (f32[144,8]{0,1:T(8,128)S(1)}, f32[144,8]{0,1:T(8,128)}, u32[]{:S(2)}) copy-start(f32[144,8]{0,1:T(8,128)} %param.16) | copy-start | bytes 13828
  14.2 8.7 %copy-start.7 = (s32[144,8]{0,1:T(8,128)S(1)}, s32[144,8]{0,1:T(8,128)}, u32[]{:S(2)}) copy-start(s32[144,8]{0,1:T(8,128)} %param.15) | copy-start | bytes 13828
  14.2 8.8 %copy-start.8 = (bf16[2048]{0:T(1024)(128)(2,1)S(1)}, bf16[2048]{0:T(1024)(128)(2,1)}, u32[]{:S(2)}) copy-start(bf16[2048]{0:T(1024)(128)(2,1)} %param.25) | copy-start | bytes 12292
  14.2 8.8 %copy-start.2 = (bf16[144,2048]{1,0:T(8,128)(2,1)S(1)}, bf16[144,2048]{1,0:T(8,128)(2,1)}, u32[]{:S(2)}) copy-start(bf16[144,2048]{1,0:T(8,128)(2,1)} %fusion.34) | copy-start | bytes 1769476
  15.2 83.1 %all-to-all-start = ((bf16[2,256,8,128]{1,3,0,2:T(8,128)(2,1)}), bf16[2,256,8,128]{1,3,0,2:T(8,128)(2,1)S(1)}, u32[]{:S(2)}, u32[]{:S(2)}) async-start(bf16[2,256,8,128]{1,3,0,2:T(8,128)(2,1)} %copy.40), calls=%async_computation | async-start | bytes 2097152 | tf_op jit(solution)/shard_map/all_to_all | solution.py:88
  21.3 256.8 %reduce-scatter.2.cloned.1.call-start = ((), (), s32[]{:S(2)}) async-start(), calls=%async_computation.3 | async-start | bytes 5308416 | tf_op jit(solution)/shard_map/reduce_scatter | solution.py:114
  21.3 78.4 %collective-permute-start.7 = (bf16[256,2048]{1,0:T(8,128)(2,1)}, bf16[256,2048]{1,0:T(8,128)(2,1)}, u32[]{:S(2)}, u32[]{:S(2)}) collective-permute-start(bf16[256,2048]{1,0:T(8,128)(2,1)} %bitcast.5), channel_id=1, source_target_pairs={{0,2},{1,3},{2,0},{3,1},{4,6},{5,7},{6,4},{7,5},{8,10},{9,11},{10,... | collective-permute-start | bytes 3145736 | tf_op jit(solution)/shard_map/ppermute | solution.py:20
  88.1 11.8 %collective-permute-start.4 = (bf16[256,2048]{1,0:T(8,128)(2,1)}, bf16[256,2048]{1,0:T(8,128)(2,1)}, u32[]{:S(2)}, u32[]{:S(2)}) collective-permute-start(bf16[256,2048]{1,0:T(8,128)(2,1)} %collective-permute-done.3), channel_id=1, source_target_pairs={{0,1},{1,0},{2,3},{3,2},{4,5},{5,4},{6,7},{7,6},{8,9},{9,8},{10,11... | collective-permute-start | bytes 3145736 | tf_op jit(solution)/shard_map/ppermute | solution.py:31
  99.3 53.8 %collective-permute-start.2 = (bf16[256,2048]{1,0:T(8,128)(2,1)}, bf16[256,2048]{1,0:T(8,128)(2,1)}, u32[]{:S(2)}, u32[]{:S(2)}) collective-permute-start(bf16[256,2048]{1,0:T(8,128)(2,1)} %bitcast.5), channel_id=1, source_target_pairs={{0,1},{1,0},{2,3},{3,2},{4,5},{5,4},{6,7},{7,6},{8,9},{9,8},{10,11... | collective-permute-start | bytes 3145736 | tf_op jit(solution)/shard_map/ppermute | solution.py:31
  99.7 66.9 %collective-permute-start.6 = (bf16[256,2048]{1,0:T(8,128)(2,1)}, bf16[256,2048]{1,0:T(8,128)(2,1)S(1)}, u32[]{:S(2)}, u32[]{:S(2)}) collective-permute-start(bf16[256,2048]{1,0:T(8,128)(2,1)} %collective-permute-done.5), channel_id=1, source_target_pairs={{0,1},{1,0},{2,3},{3,2},{4,5},{5,4},{6,7},{7,6},{8,9},{9,8},{10,11... | collective-permute-start | bytes 3145736 | tf_op jit(solution)/shard_map/ppermute | solution.py:31
  99.9 66.7 %collective-permute-start.8 = (bf16[256,2048]{1,0:T(8,128)(2,1)}, bf16[256,2048]{1,0:T(8,128)(2,1)}, u32[]{:S(2)}, u32[]{:S(2)}) collective-permute-start(bf16[256,2048]{1,0:T(8,128)(2,1)} %collective-permute-done.7), channel_id=1, source_target_pairs={{0,1},{1,0},{2,3},{3,2},{4,5},{5,4},{6,7},{7,6},{8,9},{9,8},{10,11... | collective-permute-start | bytes 3145736 | tf_op jit(solution)/shard_map/ppermute | solution.py:31
  122.3 10.9 %copy-start.3 = (bf16[3,64,2048]{2,1,0:T(8,128)(2,1)S(1)}, bf16[3,64,2048]{2,1,0:T(8,128)(2,1)}, u32[]{:S(2)}) copy-start(bf16[3,64,2048]{2,1,0:T(8,128)(2,1)} %all_gather.11) | copy-start | bytes 2359300
  183.9 94.2 %copy-start.1 = (bf16[128,2048]{1,0:T(8,128)(2,1)S(1)}, bf16[128,2048]{1,0:T(8,128)(2,1)}, u32[]{:S(2)}) copy-start(bf16[128,2048]{1,0:T(8,128)(2,1)} %param.20) | copy-start | bytes 1572868
Sparse Core Ops, SparseCore 0:
  10.2 105.1 all-gather.2
  184.0 94.0 reduce-scatter.1
